TPU v7x, 256 devices: a whole 4x4x8 slice. The times are simulated.
256 devices in a mesh: fs: 16 (over y, x), tp: 16 (over z, core).
Axes of the slice: x: 4, y: 4, z: 8, core: 2. Of those that a mesh axis runs over, the one named last changes fastest.
Arguments:
- tokens: bfloat16 [32768, 2048], P(('fs', 'tp')), may hold values from -6 to 6
- norm_gain: float32 [2048], replicated, may hold values from 0.1 to 1.9
- gate_weight: bfloat16 [2048, 5632], P('fs', 'tp'), may hold values from -0.125 to 0.125
- up_weight: bfloat16 [2048, 5632], P('fs', 'tp'), may hold values from -0.125 to 0.125
- down_weight: bfloat16 [5632, 2048], P('tp', 'fs'), may hold values from -0.078125 to 0.078125
Outputs:
- mixed: bfloat16 [32768, 2048], P(('fs', 'tp'))
All inputs are finite; a program needn't handle non-finite values.
Results may differ from a plain program's by a relative error of at most 0.0065.
Values may be sent and summed in bfloat16 or wider, within the bound.
A program may use at most 128 MiB of HBM per device.

v0:
```python
import jax
import jax.numpy as jnp
from jax import lax
from jax.sharding import PartitionSpec as P

eps_floor = 0.05


def sent_together(arrays, axis, dim, along):
    both = jnp.concatenate(arrays, axis=along)
    out, at, outs = (lax.all_gather(both, axis, axis=dim, tiled=True), 0, [])
    for a in arrays:
        outs.append(lax.slice_in_dim(out, at, at + a.shape[along], axis=along))
        at += a.shape[along]
    return tuple(outs)


def joined_along(blocks, dim):
    blocks = jnp.moveaxis(blocks, 0, dim)
    lengths = blocks.shape
    return blocks.reshape(*lengths[:dim], lengths[dim] * lengths[dim + 1], *lengths[dim + 2 :])


def from_everyone(x, axis):
    length = lax.axis_size(axis)
    return lax.all_to_all(jnp.broadcast_to(x[None], (length, *x.shape)), axis, 0, 0, tiled=True)


def collect(x, axis, dim):
    return joined_along(from_everyone(x, axis), dim)


def local(tokens, norm_gain, gate_weight, up_weight, down_weight):
    values = tokens.astype(jnp.float32)
    factor = lax.rsqrt(jnp.mean(values * values, axis=-1, keepdims=True) + eps_floor)
    normed = (values * factor * norm_gain).astype(jnp.bfloat16)
    gate_full, upper_full = sent_together((gate_weight, up_weight), "fs", 0, 1)
    piece = lax.all_gather(normed, "tp", axis=0, tiled=True)
    gate = jnp.dot(piece, gate_full, preferred_element_type=jnp.float32)
    upper = jnp.dot(piece, upper_full, preferred_element_type=jnp.float32)
    hidden = (jax.nn.silu(gate) * upper).astype(jnp.bfloat16)
    down_local = collect(down_weight, "fs", 1)
    mixed = lax.psum_scatter(
        jnp.dot(hidden, down_local, preferred_element_type=jnp.float32),
        "tp",
        scatter_dimension=0,
        tiled=True,
    )
    return mixed.astype(jnp.bfloat16)


def solution(mesh):
    return jax.shard_map(
        local,
        mesh=mesh,
        in_specs=(P(("fs", "tp"), None), P(), P("fs", "tp"), P("fs", "tp"), P("tp", "fs")),
        out_specs=P(("fs", "tp"), None),
        check_vma=False,
    )
```

profile of v0, /device:TPU:2, one launch (start us, length us, event | category | flops | bytes accessed | tf_op | source)
XLA Modules:
  0.0 261.6 jit_solution(3198704871677870176)
XLA Ops:
  6.5 0.0 all-gather.5.cloned.1.call-start
  6.5 1.6 pad_maximum_fusion
  8.1 0.0 all-gather.5.cloned.1.call-update
  8.2 0.0 all-gather.3.cloned.1.call-start
  8.2 1.2 fusion.7
  9.5 2.0 fusion.9
  11.5 0.0 all-gather.3.cloned.1.call-update
  11.5 2.2 broadcast_in_dim.2
  13.7 7.5 %all-to-all-start = ((bf16[16,352,128]{2,1,0:T(8,128)(2,1)}), bf16[16,352,128]{2,1,0:T(8,128)(2,1)S(1)}, u32[]{:S(2)}, u32[]{:S(2)}) async-start(bf16[16,352,128]{2,1,0:T(8,128)(2,1)} %broadcast_in_dim.2), calls=%async_computation | async-start | bytes 2883584 | tf_op jit(solution)/shard_map/all_to_all | solution.py:26
  21.2 0.0 reduce-scatter.2.cloned.1.call-start
  21.2 56.4 %all-gather.5.cloned.1.call-done = bf16[2048,704]{0,1:T(8,128)(2,1)} async-done(((bf16[128,704]{0,1:T(8,128)(2,1)}), bf16[2048,704]{0,1:T(8,128)(2,1)}) %all-gather.5.cloned.1.call-update) | async-done | bytes 2883600 | tf_op jit(solution)/shard_map/all_gather | solution.py:11
  77.6 57.4 %all-gather.3.cloned.1.call-done = bf16[2048,2048]{1,0:T(8,128)(2,1)} async-done(((bf16[128,2048]{1,0:T(8,128)(2,1)}), bf16[2048,2048]{1,0:T(8,128)(2,1)}) %all-gather.3.cloned.1.call-update) | async-done | bytes 8388624 | tf_op jit(solution)/shard_map/all_gather | solution.py:38
  135.0 0.0 copy-start
  135.0 0.0 copy-start.1
  135.0 6.4 %fusion.5 = f32[2048,352]{0,1:T(8,128)S(1)} fusion(bf16[2048,2048]{1,0:T(8,128)(2,1)} %all-gather.3.cloned.1.call-done, bf16[2048,704]{0,1:T(8,128)(2,1)} %all-gather.5.cloned.1.call-done), kind=kOutput, calls=%fused_computation.6 | convolution fusion | flops 2952790016 | bytes 12713984 | tf_op jit(solution)/shard_map/dot_general | solution.py:39
  141.5 0.0 copy-done
  141.5 0.6 copy-done.1
  142.1 3.5 %fusion = bf16[2048,352]{0,1:T(8,128)(2,1)S(1)} fusion(bf16[2048,2048]{1,0:T(8,128)(2,1)S(1)} %copy-done, f32[2048,352]{0,1:T(8,128)S(1)} %fusion.5, bf16[2048,704]{0,1:T(8,128)(2,1)S(1)} %copy-done.1), kind=kOutput, calls=%fused_computation.1 | convolution fusion | flops 2957115392 | bytes 14155776 | tf_op jit(solution)/shard_map/dot_general | solution.py:40
  145.6 0.0 all-to-all-done
  145.6 8.1 %fusion.1 = f32[2048,2048]{1,0:T(8,128)} fusion(bf16[2048,352]{0,1:T(8,128)(2,1)S(1)} %fusion, bf16[16,352,128]{2,1,0:T(8,128)(2,1)S(1)} %all-to-all-done), kind=kOutput, calls=%fused_computation.2 | convolution fusion | flops 2952790016 | bytes 19660800 | tf_op jit(solution)/shard_map/dot_general | solution.py:44
  153.7 0.0 reduce-scatter.2.cloned.1.call-update
  153.8 99.3 %reduce-scatter.2.cloned.1.call-done = f32[128,2048]{1,0:T(8,128)} async-done(((f32[2048,2048]{1,0:T(8,128)}), f32[128,2048]{1,0:T(8,128)}) %reduce-scatter.2.cloned.1.call-update) | async-done | bytes 1048592 | tf_op jit(solution)/shard_map/reduce_scatter | solution.py:43
  253.0 2.1 convert_element_type.15
  (1 shorter events, 0.0 us)
Async XLA Ops:
  6.5 71.1 %all-gather.5.cloned.1.call-start = ((), (), s32[]{:S(2)}) async-start(), calls=%async_computation.3 | async-start | bytes 3063808 | tf_op jit(solution)/shard_map/all_gather | solution.py:11
  8.2 126.8 %all-gather.3.cloned.1.call-start = ((), (), s32[]{:S(2)}) async-start(), calls=%async_computation.2 | async-start | bytes 8912896 | tf_op jit(solution)/shard_map/all_gather | solution.py:38
  13.7 131.9 %all-to-all-start = ((bf16[16,352,128]{2,1,0:T(8,128)(2,1)}), bf16[16,352,128]{2,1,0:T(8,128)(2,1)S(1)}, u32[]{:S(2)}, u32[]{:S(2)}) async-start(bf16[16,352,128]{2,1,0:T(8,128)(2,1)} %broadcast_in_dim.2), calls=%async_computation | async-start | bytes 2883584 | tf_op jit(solution)/shard_map/all_to_all | solution.py:26
  21.2 231.8 %reduce-scatter.2.cloned.1.call-start = ((), (), s32[]{:S(2)}) async-start(), calls=%async_computation.4 | async-start | bytes 17825792 | tf_op jit(solution)/shard_map/reduce_scatter | solution.py:43
  135.0 6.4 %copy-start = (bf16[2048,2048]{1,0:T(8,128)(2,1)S(1)}, bf16[2048,2048]{1,0:T(8,128)(2,1)}, u32[]{:S(2)}) copy-start(bf16[2048,2048]{1,0:T(8,128)(2,1)} %all-gather.3.cloned.1.call-done) | copy-start | bytes 25165828
  135.0 7.1 %copy-start.1 = (bf16[2048,704]{0,1:T(8,128)(2,1)S(1)}, bf16[2048,704]{0,1:T(8,128)(2,1)}, u32[]{:S(2)}) copy-start(bf16[2048,704]{0,1:T(8,128)(2,1)} %all-gather.5.cloned.1.call-done) | copy-start | bytes 8650756
Sparse Core Ops, SparseCore 0:
  9.7 67.8 all-gather.4
  79.4 55.5 all-gather.2
  153.9 99.0 reduce-scatter.1
where the time goes:
time: 262 us
  waiting for transfers between devices  213 us (81%)
  matrix products  18.1 us (7%)
  between operations  13.1 us (5%)
  starting transfers between devices  7.56 us (3%)
  other arithmetic  6.96 us (3%)
  local copies, waits for them, and re-layouts  2.83 us (1%)
    reduce_scatter x1, waiting for transfers between devices, local(): lax.psum_scatter(jnp.dot(hidden, down_local, preferred_element_type=jnp.f...  99.3 us
    all_gather x1, waiting for transfers between devices, local(): piece = lax.all_gather(normed, 'tp', axis=0, tiled=True)  57.4 us
    all_gather x1, waiting for transfers between devices, sent_together(): out, at, outs = (lax.all_gather(both, axis, axis=dim, tiled=True), 0, [])  56.4 us
    dot_general x1, matrix products, local(): jnp.dot(hidden, down_local, preferred_element_type=jnp.float32)  8.11 us
    all_to_all x1, starting transfers between devices, from_everyone(): lax.all_to_all(jnp.broadcast_to(x[None], (length, *x.shape)), axis, 0, 0,...  7.48 us
    dot_general x1, matrix products, local(): gate = jnp.dot(piece, gate_full, preferred_element_type=jnp.float32)  6.43 us
  transfers between devices with their start and end apart: 4, of which 3 were waited for; matrix products, arithmetic and copies ran while one was open for 6% of the time, Pallas kernels for 0%

commit v1 on v0

--- a/solution.py
+++ b/solution.py
@@ -35,7 +35,8 @@
     factor = lax.rsqrt(jnp.mean(values * values, axis=-1, keepdims=True) + eps_floor)
     normed = (values * factor * norm_gain).astype(jnp.bfloat16)
     gate_full, upper_full = sent_together((gate_weight, up_weight), "fs", 0, 1)
-    piece = lax.all_gather(normed, "tp", axis=0, tiled=True)
+    sent = jnp.stack([normed] * lax.axis_size("tp"))
+    piece = jnp.concatenate(lax.all_to_all(sent, "tp", 0, 0), axis=0)
     gate = jnp.dot(piece, gate_full, preferred_element_type=jnp.float32)
     upper = jnp.dot(piece, upper_full, preferred_element_type=jnp.float32)
     hidden = (jax.nn.silu(gate) * upper).astype(jnp.bfloat16)

time: 262 us -> 351 us (1.34)
  waiting for transfers between devices: 213 us -> 289 us
  starting transfers between devices: 7.56 us -> 16.3 us
    all_to_all x0 -> x1, waiting for transfers between devices: none -> 183 us  [local(): piece = jnp.concatenate(lax.all_to_all(sent, 'tp', 0, 0), axis=0)]
    all_gather x1 -> x0, waiting for transfers between devices: 57.4 us -> none  [local(): piece = lax.all_gather(normed, 'tp', axis=0, tiled=True)]
    all_gather x1, waiting for transfers between devices: 56.4 us -> 0.02 us  [sent_together(): out, at, outs = (lax.all_gather(both, axis, axis=dim, tiled=True), 0, [])]
    all_to_all x0 -> x1, starting transfers between devices: none -> 8.75 us  [local(): piece = jnp.concatenate(lax.all_to_all(sent, 'tp', 0, 0), axis=0)]
    all_to_all x1, waiting for transfers between devices: 0.01 us -> 6.68 us  [from_everyone(): lax.all_to_all(jnp.broadcast_to(x[None], (length, *x.shape)), axis, 0, 0,...]
    another operation x0 -> x1, local copies, waits for them, and re-layouts: none -> 4.31 us  [local(): sent = jnp.stack([normed] * lax.axis_size('tp'))]
  transfers between devices with their start and end apart: 4 -> 4, of which waited for: 3 -> 3; matrix products, arithmetic and copies ran while one was open for 6% -> 4% of each run, Pallas kernels for 0% -> 0%
where the time goes in v1:
time: 351 us
  waiting for transfers between devices  289 us (82%)
  matrix products  21.2 us (6%)
  starting transfers between devices  16.3 us (5%)
  between operations  13.5 us (4%)
  local copies, waits for them, and re-layouts  5.68 us (2%)
  other arithmetic  5.24 us (1%)
    all_to_all x1, waiting for transfers between devices, local(): piece = jnp.concatenate(lax.all_to_all(sent, 'tp', 0, 0), axis=0)  183 us
    reduce_scatter x1, waiting for transfers between devices, local(): lax.psum_scatter(jnp.dot(hidden, down_local, preferred_element_type=jnp.f...  98.6 us
    all_to_all x1, starting transfers between devices, local(): piece = jnp.concatenate(lax.all_to_all(sent, 'tp', 0, 0), axis=0)  8.75 us
    dot_general x1, matrix products, local(): jnp.dot(hidden, down_local, preferred_element_type=jnp.float32)  8.18 us
    all_to_all x1, starting transfers between devices, from_everyone(): lax.all_to_all(jnp.broadcast_to(x[None], (length, *x.shape)), axis, 0, 0,...  7.48 us
  transfers between devices with their start and end apart: 4, of which 3 were waited for; matrix products, arithmetic and copies ran while one was open for 4% of the time, Pallas kernels for 0%

profile of v1, /device:TPU:2, one launch (start us, length us, event | category | flops | bytes accessed | tf_op | source)
XLA Modules:
  0.0 350.7 jit_solution(3526202078781301542)
XLA Ops:
  6.5 1.2 fusion.7
  7.8 1.2 fusion.9
  9.0 4.3 %stack.2 = bf16[16,128,2048]{2,1,0:T(8,128)(2,1)} broadcast(bf16[128,2048]{1,0:T(8,128)(2,1)S(1)} %fusion.9), dimensions={1,2} | broadcast | bytes 8912896 | tf_op jit(solution)/shard_map/stack | solution.py:38
  13.3 0.0 copy-start
  13.3 0.0 copy-start.1
  13.3 0.0 copy-start.2
  13.3 8.8 %all-to-all-start = ((bf16[16,128,2048]{2,1,0:T(8,128)(2,1)}), bf16[16,128,2048]{2,1,0:T(8,128)(2,1)}, u32[]{:S(2)}, u32[]{:S(2)}) async-start(bf16[16,128,2048]{2,1,0:T(8,128)(2,1)} %stack.2), calls=%async_computation | async-start | bytes 16777216 | tf_op jit(solution)/shard_map/all_to_all | solution.py:39
  22.1 0.0 all-gather.2.cloned.1.call-start
  22.1 0.0 copy-done
  22.1 0.0 copy-done.1
  22.2 0.7 pad_maximum_fusion
  22.8 0.0 all-gather.2.cloned.1.call-update
  22.9 183.4 %all-to-all-done = bf16[16,128,2048]{2,1,0:T(8,128)(2,1)} async-done(((bf16[16,128,2048]{2,1,0:T(8,128)(2,1)}), bf16[16,128,2048]{2,1,0:T(8,128)(2,1)}, u32[]{:S(2)}, u32[]{:S(2)}) %all-to-all-start) | async-done | bytes 8388640 | tf_op jit(solution)/shard_map/all_to_all | solution.py:39
  206.3 0.0 copy-done.2
  206.3 1.4 broadcast_in_dim.2
  207.7 7.5 %all-to-all-start.1 = ((bf16[16,352,128]{2,1,0:T(8,128)(2,1)}), bf16[16,352,128]{2,1,0:T(8,128)(2,1)S(1)}, u32[]{:S(2)}, u32[]{:S(2)}) async-start(bf16[16,352,128]{2,1,0:T(8,128)(2,1)} %broadcast_in_dim.2), calls=%async_computation.1 | async-start | bytes 2883584 | tf_op jit(solution)/shard_map/all_to_all | solution.py:26
  215.1 0.0 reduce-scatter.2.cloned.1.call-start
  215.2 0.0 all-gather.2.cloned.1.call-done
  215.2 0.0 copy-start.3
  215.2 6.2 %fusion.5 = f32[2048,352]{0,1:T(8,128)S(1)} fusion(bf16[2048,2048]{1,0:T(8,128)(2,1)} %bitcast, bf16[2048,704]{0,1:T(8,128)(2,1)} %all-gather.2.cloned.1.call-done), kind=kOutput, calls=%fused_computation.6 | convolution fusion | flops 2952790016 | bytes 12713984 | tf_op jit(solution)/shard_map/dot_general | solution.py:40
  221.4 0.0 copy-done.3
  221.4 6.8 %fusion = bf16[2048,352]{0,1:T(8,128)(2,1)S(1)} fusion(bf16[2048,2048]{1,0:T(8,128)(2,1)} %bitcast, f32[2048,352]{0,1:T(8,128)S(1)} %fusion.5, bf16[2048,704]{0,1:T(8,128)(2,1)S(1)} %copy-done.3), kind=kOutput, calls=%fused_computation.1 | convolution fusion | flops 2957115392 | bytes 14155776 | tf_op jit(solution)/shard_map/dot_general | solution.py:41
  228.3 6.7 %all-to-all-done.1 = bf16[16,352,128]{2,1,0:T(8,128)(2,1)S(1)} async-done(((bf16[16,352,128]{2,1,0:T(8,128)(2,1)}), bf16[16,352,128]{2,1,0:T(8,128)(2,1)S(1)}, u32[]{:S(2)}, u32[]{:S(2)}) %all-to-all-start.1) | async-done | bytes 1441824 | tf_op jit(solution)/shard_map/all_to_all | solution.py:26
  234.9 8.2 %fusion.1 = f32[2048,2048]{1,0:T(8,128)} fusion(bf16[2048,352]{0,1:T(8,128)(2,1)S(1)} %fusion, bf16[16,352,128]{2,1,0:T(8,128)(2,1)S(1)} %all-to-all-done.1), kind=kOutput, calls=%fused_computation.2 | convolution fusion | flops 2952790016 | bytes 19660800 | tf_op jit(solution)/shard_map/dot_general | solution.py:45
  243.1 0.0 reduce-scatter.2.cloned.1.call-update
  243.1 98.6 %reduce-scatter.2.cloned.1.call-done = f32[128,2048]{1,0:T(8,128)} async-done(((f32[2048,2048]{1,0:T(8,128)}), f32[128,2048]{1,0:T(8,128)}) %reduce-scatter.2.cloned.1.call-update) | async-done | bytes 1048592 | tf_op jit(solution)/shard_map/reduce_scatter | solution.py:44
  341.8 2.1 convert_element_type.15
  (1 shorter events, 0.0 us)
Async XLA Ops:
  13.3 8.8 %copy-start = (bf16[128,352]{0,1:T(8,128)(2,1)S(1)}, bf16[128,352]{0,1:T(8,128)(2,1)}, u32[]{:S(2)}) copy-start(bf16[128,352]{0,1:T(8,128)(2,1)} %param.8) | copy-start | bytes 270340
  13.3 8.8 %copy-start.1 = (bf16[128,352]{0,1:T(8,128)(2,1)S(1)}, bf16[128,352]{0,1:T(8,128)(2,1)}, u32[]{:S(2)}) copy-start(bf16[128,352]{0,1:T(8,128)(2,1)} %param.7) | copy-start | bytes 270340
  13.3 193.0 %copy-start.2 = (bf16[352,128]{1,0:T(8,128)(2,1)S(1)}, bf16[352,128]{1,0:T(8,128)(2,1)}, u32[]{:S(2)}) copy-start(bf16[352,128]{1,0:T(8,128)(2,1)} %param.9) | copy-start | bytes 270340
  13.3 193.0 %all-to-all-start = ((bf16[16,128,2048]{2,1,0:T(8,128)(2,1)}), bf16[16,128,2048]{2,1,0:T(8,128)(2,1)}, u32[]{:S(2)}, u32[]{:S(2)}) async-start(bf16[16,128,2048]{2,1,0:T(8,128)(2,1)} %stack.2), calls=%async_computation | async-start | bytes 16777216 | tf_op jit(solution)/shard_map/all_to_all | solution.py:39
  22.1 193.1 %all-gather.2.cloned.1.call-start = ((), (), s32[]{:S(2)}) async-start(), calls=%async_computation.3 | async-start | bytes 3063808 | tf_op jit(solution)/shard_map/all_gather | solution.py:11
  207.7 27.3 %all-to-all-start.1 = ((bf16[16,352,128]{2,1,0:T(8,128)(2,1)}), bf16[16,352,128]{2,1,0:T(8,128)(2,1)S(1)}, u32[]{:S(2)}, u32[]{:S(2)}) async-start(bf16[16,352,128]{2,1,0:T(8,128)(2,1)} %broadcast_in_dim.2), calls=%async_computation.1 | async-start | bytes 2883584 | tf_op jit(solution)/shard_map/all_to_all | solution.py:26
  215.1 126.6 %reduce-scatter.2.cloned.1.call-start = ((), (), s32[]{:S(2)}) async-start(), calls=%async_computation.4 | async-start | bytes 17825792 | tf_op jit(solution)/shard_map/reduce_scatter | solution.py:44
  215.2 6.2 %copy-start.3 = (bf16[2048,704]{0,1:T(8,128)(2,1)S(1)}, bf16[2048,704]{0,1:T(8,128)(2,1)}, u32[]{:S(2)}) copy-start(bf16[2048,704]{0,1:T(8,128)(2,1)} %all-gather.2.cloned.1.call-done) | copy-start | bytes 8650756
Sparse Core Ops, SparseCore 0:
  25.3 56.8 all-gather.1
  243.3 98.4 reduce-scatter.1
